TPU v7x, 32 devices: a whole 2x2x4 slice. The times are simulated.
32 devices in a mesh: ep: 16 (over z, y, x), tp: 2 (over core).
Axes of the slice: x: 2, y: 2, z: 4, core: 2. Of those that a mesh axis runs over, the one named last changes fastest.
Arguments:
- tokens: bfloat16 [384, 2048], P('ep'), may hold values from -6 to 6
- norm_gain: bfloat16 [2048], replicated, may hold values from 0.099609375 to 1.8984375
- query_w: bfloat16 [2048, 1024], P(None, 'tp'), may hold values from -0.125 to 0.125
- key_w: bfloat16 [2048, 128], replicated, may hold values from -0.125 to 0.125
- value_w: bfloat16 [2048, 128], replicated, may hold values from -0.125 to 0.125
- forget_w: bfloat16 [2048, 16], replicated, may hold values from -0.125 to 0.125
- forget_bias: float32 [16], replicated, may hold values from 0 to 4
- query_gain: bfloat16 [64], replicated, may hold values from 0.099609375 to 1.8984375
- key_gain: bfloat16 [64], replicated, may hold values from 0.099609375 to 1.8984375
- cache_key: bfloat16 [384, 2, 64, 1024], P('ep', 'tp'), may hold values from -6 to 6
- cache_value: bfloat16 [384, 2, 64, 1024], P('ep', 'tp'), may hold values from -6 to 6
- cache_gate: float32 [384, 16, 1024], P('ep', 'tp'), may hold values from -105 to 0, as said below
- cache_len: int32 [384], P('ep'), may hold values from 256 to 1024
- out_w: bfloat16 [1024, 2048], P('tp'), may hold values from -0.1875 to 0.1875
- post_gain: bfloat16 [2048], replicated, may hold values from 0.099609375 to 1.8984375
- branch_gate: bfloat16 [2048], replicated, may hold values from -0.125 to 0.125
- dense_gate_w: bfloat16 [2048, 16384], P(None, ('ep', 'tp')), may hold values from -0.125 to 0.125
- dense_up_w: bfloat16 [2048, 16384], P(None, ('ep', 'tp')), may hold values from -1.3258252 to 1.3258252
- dense_down_w: bfloat16 [16384, 2048], P(('ep', 'tp')), may hold values from -0.046875 to 0.046875
- expert_choice: int32 [384, 2], P('ep'), may hold values from 0 to 15, as said below
- route_weight: float32 [384, 2], P('ep'), may hold values from 0.1 to 1
- expert_gate_w: bfloat16 [16, 2048, 1024], P('ep', None, 'tp'), may hold values from -0.125 to 0.125
- expert_up_w: bfloat16 [16, 2048, 1024], P('ep', None, 'tp'), may hold values from -0.125 to 0.125
- expert_down_w: bfloat16 [16, 1024, 2048], P('ep', 'tp'), may hold values from -0.1875 to 0.1875
Outputs:
- mixed_out: bfloat16 [384, 2048], P('ep', 'tp')
- fresh_key: bfloat16 [384, 2, 64], P('ep', 'tp')
- fresh_value: bfloat16 [384, 2, 64], P('ep', 'tp')
- fresh_gate: float32 [384, 16], P('ep', 'tp')
Inputs may be any that keep to these rules, and one draw needn't show every extreme that they name: `cache_gate`: Non-increasing along positions. `expert_choice`: experts 4 * g to 4 * g + 3 form group g. A token names 2 different experts of one group. Among the 24 tokens of one index of ep, those at even offsets all choose one group and the others choose other groups; no expert is named more than 6 times by them, and some expert exactly 6 times.
All inputs are finite; a program needn't handle non-finite values.
Results may differ from a plain program's by a relative error of at most 0.014.
Values may be sent and summed in bfloat16 or wider, within the bound.
A program may use at most 128 MiB of HBM per device.

v0:
```python
import jax
import jax.numpy as jnp
from jax import lax
from jax.sharding import PartitionSpec as P

FF2 = 16384
GROUPS = 4


norm_eps = 1e-06


def rms_scale(values, gain_vec):
    mean_square = jnp.mean(values * values, axis=-1, keepdims=True)
    return values * lax.rsqrt(mean_square + norm_eps) * gain_vec


def rounded(values):
    return lax.optimization_barrier(values.astype(jnp.bfloat16)).astype(jnp.float32)


def swiglu_rows(inputs, gate_weight, up_weight):
    gate_value = jnp.dot(inputs, gate_weight, preferred_element_type=jnp.float32)
    up_value = jnp.dot(inputs, up_weight, preferred_element_type=jnp.float32)
    return jax.nn.silu(gate_value) * up_value


def flat_terms(hidden, down_weight, ep_count, tp_count, seq_count):
    spread_hidden = hidden.astype(jnp.bfloat16).reshape(ep_count, seq_count, -1)
    split_down = down_weight.reshape(down_weight.shape[0], tp_count, -1)
    return jnp.einsum(
        "esh,hcd->ecsd", spread_hidden, split_down, preferred_element_type=jnp.float32
    )


def body(
    tokens,
    norm_gain,
    query_w,
    key_w,
    value_w,
    forget_w,
    forget_bias,
    query_gain,
    key_gain,
    cache_key,
    cache_value,
    cache_gate,
    cache_len,
    out_w,
    post_gain,
    branch_gate,
    dense_gate_w,
    dense_up_w,
    dense_down_w,
    expert_choice,
    route_weight,
    expert_gate_w,
    expert_up_w,
    expert_down_w,
):
    seq_count = tokens.shape[0]
    model_width = tokens.shape[1]
    heads_local = cache_gate.shape[1]
    kv_local = cache_key.shape[1]
    head_size = cache_key.shape[2]
    cache_span = cache_key.shape[3]
    tp_count = lax.axis_size("tp")
    ep_count = lax.axis_size("ep")
    tp_rank = lax.axis_index("tp")
    half_width = model_width // tp_count
    score_scale = head_size ** (-0.5)
    resid_in = tokens.astype(jnp.float32)
    normed = rms_scale(resid_in, norm_gain.astype(jnp.float32)).astype(jnp.bfloat16)
    queries = jnp.dot(normed, query_w, preferred_element_type=jnp.float32).reshape(
        seq_count, heads_local, head_size
    )
    queries = rms_scale(queries, query_gain.astype(jnp.float32)).astype(jnp.bfloat16)
    keys_all = jnp.dot(normed, key_w, preferred_element_type=jnp.float32).reshape(
        seq_count, -1, head_size
    )
    keys_all = rms_scale(keys_all, key_gain.astype(jnp.float32)).astype(jnp.bfloat16)
    values_all = (
        jnp.dot(normed, value_w, preferred_element_type=jnp.float32)
        .astype(jnp.bfloat16)
        .reshape(seq_count, -1, head_size)
    )
    fresh_key = lax.dynamic_slice_in_dim(keys_all, tp_rank * kv_local, kv_local, 1)
    fresh_value = lax.dynamic_slice_in_dim(values_all, tp_rank * kv_local, kv_local, 1)
    forget_all = jax.nn.log_sigmoid(
        jnp.dot(normed, forget_w, preferred_element_type=jnp.float32) + forget_bias
    )
    log_forget = lax.dynamic_slice_in_dim(forget_all, tp_rank * heads_local, heads_local, 1)
    repeat = heads_local // kv_local
    grouped = queries.reshape(seq_count, kv_local, repeat, head_size)
    scores = (
        jnp.einsum("sgrd,sgdl->sgrl", grouped, cache_key, preferred_element_type=jnp.float32)
        * score_scale
    )
    own_score = (
        jnp.einsum("sgrd,sgd->sgr", grouped, fresh_key, preferred_element_type=jnp.float32)
        * score_scale
    )
    current_slot_offset = lax.broadcasted_iota(jnp.int32, (seq_count, cache_span), 1)
    at_last = (current_slot_offset == cache_len[:, None] - 1)[:, None, :]
    previous = jnp.sum(jnp.where(at_last, cache_gate, jnp.zeros_like(cache_gate)), axis=2)
    current = previous + log_forget
    decay_bias = (current[:, :, None] - cache_gate).reshape(seq_count, kv_local, repeat, cache_span)
    is_valid = (current_slot_offset < cache_len[:, None])[:, None, None, :]
    logits = jnp.where(is_valid, scores + decay_bias, -jnp.inf)
    top_logit = jnp.maximum(jnp.max(logits, axis=3), own_score)
    weights = jnp.exp(logits - top_logit[..., None])
    own_weight = jnp.exp(own_score - top_logit)
    total_weight = jnp.sum(weights, axis=3) + own_weight
    cache_probs = (weights / total_weight[..., None]).astype(jnp.bfloat16)
    own_prob = (own_weight / total_weight).astype(jnp.bfloat16)
    mixed_heads = jnp.einsum(
        "sgrl,sgdl->sgrd", cache_probs, cache_value, preferred_element_type=jnp.float32
    )
    mixed_heads = (
        mixed_heads
        + own_prob.astype(jnp.float32)[..., None] * fresh_value.astype(jnp.float32)[:, :, None, :]
    )
    attn_heads = mixed_heads.reshape(seq_count, heads_local * head_size).astype(jnp.bfloat16)
    partial_value = jnp.dot(attn_heads, out_w, preferred_element_type=jnp.float32)
    attn_sum = lax.psum(partial_value.astype(jnp.bfloat16), "tp").astype(jnp.float32)
    resid_out = rounded(resid_in + attn_sum)
    post_norm = rms_scale(resid_out, post_gain.astype(jnp.float32)).astype(jnp.bfloat16)
    branch = jax.nn.sigmoid(jnp.dot(post_norm, branch_gate, preferred_element_type=jnp.float32))
    all_tokens = lax.all_gather(post_norm, "ep", axis=0, tiled=True)
    hidden = swiglu_rows(all_tokens, dense_gate_w, dense_up_w)
    squares = jnp.sum(hidden * hidden, axis=1)
    dense_terms = flat_terms(hidden, dense_down_w, ep_count, tp_count, seq_count)
    spread = jnp.broadcast_to(
        squares.reshape(ep_count, 1, seq_count), (ep_count, tp_count, seq_count)
    ).reshape(-1)
    dense_sum, square_sum = (
        lax.psum_scatter(
            dense_terms.reshape(-1, half_width), ("ep", "tp"), scatter_dimension=0, tiled=True
        ),
        lax.psum_scatter(spread, ("ep", "tp"), scatter_dimension=0, tiled=True),
    )
    dense_out = rounded(dense_sum * lax.rsqrt(square_sum / FF2 + norm_eps)[:, None])
    per_group = ep_count // GROUPS
    capacity = 2 * ((seq_count + 2 * per_group - 1) // (2 * per_group))
    route_count = expert_choice.shape[1]
    route_ids = expert_choice.reshape(-1)
    member = (route_ids[:, None] == jnp.arange(ep_count)[None, :]).astype(jnp.int32)
    slot_index = jnp.sum((jnp.cumsum(member, axis=0) - member) * member, axis=1)
    target = (route_ids * capacity + slot_index).reshape(seq_count, route_count)
    place_map = (target[:, :, None] == jnp.arange(ep_count * capacity)[None, None, :]).astype(
        jnp.bfloat16
    )
    outgoing = jnp.einsum("skc,sd->cd", place_map, post_norm, preferred_element_type=jnp.float32)
    outgoing = outgoing.astype(jnp.bfloat16).reshape(ep_count, capacity, model_width)
    arrived = lax.all_to_all(outgoing, "ep", split_axis=0, concat_axis=0, tiled=True)
    item_count = arrived.shape[1]
    slot_rows = arrived.reshape(-1, model_width)
    activated = swiglu_rows(slot_rows, expert_gate_w[0], expert_up_w[0]).astype(jnp.bfloat16)
    partial_out = jnp.dot(activated, expert_down_w[0], preferred_element_type=jnp.float32)
    partial_out = partial_out.reshape(ep_count, item_count, model_width)
    halves = lax.psum_scatter(
        partial_out.astype(jnp.bfloat16), "tp", scatter_dimension=2, tiled=True
    )
    returned = lax.all_to_all(halves, "ep", split_axis=0, concat_axis=0, tiled=True).reshape(
        ep_count * capacity, half_width
    )
    routed = jnp.einsum("skc,cd->skd", place_map, returned, preferred_element_type=jnp.float32)
    expert_sum = jnp.sum(route_weight[:, :, None] * routed, axis=1)
    resid_columns = lax.dynamic_slice_in_dim(resid_out, tp_rank * half_width, half_width, 1)
    mixed_out = (resid_columns + expert_sum + branch[:, None] * dense_out).astype(jnp.bfloat16)
    return (mixed_out, fresh_key, fresh_value, current)


def solution(mesh):
    placed = (
        P("ep", None),
        P(),
        P(None, "tp"),
        P(),
        P(),
        P(),
        P(),
        P(),
        P(),
        P("ep", "tp", None, None),
        P("ep", "tp", None, None),
        P("ep", "tp", None),
        P("ep"),
        P("tp", None),
        P(),
        P(),
        P(None, ("ep", "tp")),
        P(None, ("ep", "tp")),
        P(("ep", "tp"), None),
        P("ep", None),
        P("ep", None),
        P("ep", None, "tp"),
        P("ep", None, "tp"),
        P("ep", "tp", None),
    )
    return jax.shard_map(
        body,
        mesh=mesh,
        in_specs=placed,
        out_specs=(P("ep", "tp"), P("ep", "tp", None), P("ep", "tp", None), P("ep", "tp")),
        check_vma=False,
    )
```

profile of v0, /device:TPU:0, one launch (start us, length us, event | category | flops | bytes accessed | tf_op | source)
XLA Modules:
  0.0 239.2 jit_solution(11453295453262258375)
XLA Ops:
  8.1 0.9 iota_compare_fusion.1
  9.0 1.3 select_reduce_fusion
  11.1 1.0 fusion.41
  12.2 1.2 fusion.68
  13.4 2.1 fusion.66
  15.8 1.3 fusion.63
  17.7 1.9 fusion.69
  21.8 3.1 %fusion.30 = bf16[24,8,64]{2,1,0:T(8,128)(2,1)S(1)} fusion(bf16[24,1,64,1024]{3,2,1,0:T(8,128)(2,1)} %param.34, f32[24,8,1024]{2,1,0:T(8,128)} %copy-done.1, f32[24,8]{1,0:T(8,128)S(1)} %get-tuple-element.9, f32[24,8]{1,0:T(8,128)S(1)} %multiply_maximum_fusion, f32[24,64]{1,0:T(8,128)S(1)} %get-tuple-element.4, f32[24,8]{1,0:T(8,128)S(1)} %get-tuple-element.8), kind=kOutput, calls=%fused_computation.24 | convolution fusion | flops 25792512 | bytes 3965184 | tf_op jit(solution)/shard_map/sgrl,sgdl->sgrd/dot_general | solution.py:117
  25.0 2.6 %convolution_convert_fusion.2 = bf16[24,2048]{1,0:T(8,128)(2,1)} fusion(bf16[24,512]{1,0:T(8,128)(2,1)S(1)} %convert_element_type.106, bf16[512,2048]{1,0:T(8,128)(2,1)} %param.37), kind=kOutput, calls=%fused_computation.6 | convolution fusion | flops 50380800 | bytes 2220032 | tf_op jit(solution)/shard_map/dot_general | solution.py:125
  27.7 20.6 %all-reduce.3.cloned.1.call-done = bf16[24,2048]{1,0:T(8,128)(2,1)} async-done(((bf16[24,2048]{1,0:T(8,128)(2,1)}), bf16[24,2048]{1,0:T(8,128)(2,1)}) %all-reduce.3.cloned.1.call-update) | async-done | bytes 98320 | tf_op jit(solution)/shard_map/psum | solution.py:126
  48.4 0.9 fusion.44
  51.5 1.2 fusion.71
  52.7 0.9 reshape.193
  53.6 24.4 %all_to_all.10 = bf16[16,6,2048]{2,1,0:T(8,128)(2,1)} all-to-all(bf16[16,6,2048]{2,1,0:T(8,128)(2,1)} %reshape.193), channel_id=1, replica_groups=mesh['ep'=16,'tp'=2] {'ep'}, dimensions={0} | all-to-all | bytes 786432 | tf_op jit(solution)/shard_map/all_to_all | solution.py:156
  78.1 1.2 reshape.194
  79.3 2.2 fusion.9
  81.5 1.1 fusion.24
  82.6 0.9 dot_general.64
  83.5 2.8 %convolution_convert_fusion = bf16[16,6,2048]{2,0,1:T(8,128)(2,1)} fusion(bf16[1,512,2048]{2,1,0:T(8,128)(2,1)} %param.47, bf16[16,6,512]{2,1,0:T(8,128)(2,1)S(1)} %dot_general.64), kind=kOutput, calls=%fused_computation.4 | convolution fusion | flops 201523200 | bytes 2588672 | tf_op jit(solution)/shard_map/dot_general | solution.py:160
  86.4 26.2 %all-gather.2.cloned.1.call-done = bf16[384,2048]{1,0:T(8,128)(2,1)} async-done(((bf16[24,2048]{1,0:T(8,128)(2,1)}), bf16[384,2048]{1,0:T(8,128)(2,1)}) %all-gather.2.cloned.1.call-update) | async-done | bytes 1572880 | tf_op jit(solution)/shard_map/all_gather | solution.py:130
  112.6 3.2 %fusion.70 = f32[384,512]{1,0:T(8,128)S(1)} fusion(bf16[384,2048]{1,0:T(8,128)(2,1)} %all-gather.2.cloned.1.call-done, bf16[2048,512]{1,0:T(8,128)(2,1)} %param.40), kind=kOutput, calls=%fused_computation.98 | convolution fusion | flops 805306368 | bytes 4456448 | tf_op jit(solution)/shard_map/dot_general | solution.py:23
  115.8 1.1 multiply_reduce_fusion
  117.4 2.7 %fusion.4 = f32[16,24,2,1024]{3,1,2,0:T(8,128)} fusion(bf16[16,24,512,1]{2,1,3,0:T(8,128)(2,1)S(1)} %bitcast.85, bf16[64,2,8,1024]{3,2,1,0:T(8,128)(2,1)S(1)} %bitcast.84), kind=kOutput, calls=%fused_computation.8 | convolution fusion | flops 805306368 | bytes 5636096 | tf_op jit(solution)/shard_map/esh,hcd->ecsd/dot_general | solution.py:31
  121.4 1.8 copy.67
  123.1 6.8 %all-to-all-start.1 = ((bf16[16,6,1024]{2,1,0:T(8,128)(2,1)}), bf16[16,6,1024]{2,1,0:T(8,128)(2,1)S(1)}, u32[]{:S(2)}, u32[]{:S(2)}) async-start(bf16[16,6,1024]{2,1,0:T(8,128)(2,1)} %copy.67), calls=%async_computation.2 | async-start | bytes 524288 | tf_op jit(solution)/shard_map/all_to_all | solution.py:165
  131.3 1.0 fusion.37
  132.3 7.9 %all-to-all-done.1 = bf16[16,6,1024]{2,1,0:T(8,128)(2,1)S(1)} async-done(((bf16[16,6,1024]{2,1,0:T(8,128)(2,1)}), bf16[16,6,1024]{2,1,0:T(8,128)(2,1)S(1)}, u32[]{:S(2)}, u32[]{:S(2)}) %all-to-all-start.1) | async-done | bytes 196640 | tf_op jit(solution)/shard_map/all_to_all | solution.py:165
  141.0 1.2 fusion.23
  142.4 38.9 %all-reduce = f32[768]{0:T(1024)S(1)} all-reduce(f32[768]{0:T(1024)S(1)} %reshape.199), channel_id=4, replica_groups=mesh['ep'=16,'tp'=2] {'ep','tp'}, use_global_device_ids=true, to_apply=%region_15.16.clone | all-reduce | flops 768 | bytes 6144
  181.4 48.7 %reduce-scatter.5.cloned.1.call-done = f32[24,1024]{1,0:T(8,128)} async-done(((f32[768,1024]{1,0:T(8,128)}), f32[24,1024]{1,0:T(8,128)}) %reduce-scatter.5.cloned.1.call-update) | async-done | bytes 98320 | tf_op jit(solution)/shard_map/reduce_scatter | solution.py:138
  230.1 1.0 multiply_convert_fusion.1
  231.1 1.6 add_convert_fusion
  (100 shorter events, 11.3 us)
Async XLA Ops:
  7.2 10.6 %copy-start = (bf16[24,1,64,1024]{3,2,1,0:T(8,128)(2,1)S(1)}, bf16[24,1,64,1024]{3,2,1,0:T(8,128)(2,1)}, u32[]{:S(2)}) copy-start(bf16[24,1,64,1024]{3,2,1,0:T(8,128)(2,1)} %param.33) | copy-start | bytes 9437188
  7.2 8.6 %copy-start.2 = (bf16[24,2048]{1,0:T(8,128)(2,1)S(1)}, bf16[24,2048]{1,0:T(8,128)(2,1)}, u32[]{:S(2)}) copy-start(bf16[24,2048]{1,0:T(8,128)(2,1)} %param.24) | copy-start | bytes 294916
  7.2 8.4 %copy-start.19 = (bf16[64]{0:T(256)(128)(2,1)S(1)}, bf16[64]{0:T(256)(128)(2,1)}, u32[]{:S(2)}) copy-start(bf16[64]{0:T(256)(128)(2,1)} %param.31) | copy-start | bytes 388
  7.2 8.5 %copy-start.20 = (bf16[64]{0:T(256)(128)(2,1)S(1)}, bf16[64]{0:T(256)(128)(2,1)}, u32[]{:S(2)}) copy-start(bf16[64]{0:T(256)(128)(2,1)} %param.32) | copy-start | bytes 388
  7.2 41.1 %all-reduce.3.cloned.1.call-start = ((), (), s32[]{:S(2)}) async-start(), calls=%async_computation.4 | async-start | bytes 196608 | tf_op jit(solution)/shard_map/psum | solution.py:126
  13.4 6.3 %copy-start.7 = (f32[24,8]{0,1:T(8,128)}, f32[24,8]{0,1:T(8,128)S(1)}, u32[]{:S(2)}) copy-start(f32[24,8]{0,1:T(8,128)S(1)} %fusion.55) | copy-start | bytes 2308
  15.8 3.8 %copy-start.11 = (f32[64]{0:T(128)}, f32[64]{0:T(128)S(1)}, u32[]{:S(2)}) copy-start(f32[64]{0:T(128)S(1)} %convert_element_type.99) | copy-start | bytes 772
  17.4 2.2 copy-start.13
  17.7 3.1 %copy-start.6 = (bf16[2048,128]{1,0:T(8,128)(2,1)S(1)}, bf16[2048,128]{1,0:T(8,128)(2,1)}, u32[]{:S(2)}) copy-start(bf16[2048,128]{1,0:T(8,128)(2,1)} %param.28) | copy-start | bytes 1572868
  19.6 0.9 copy-start.1
  24.9 2.8 %copy-start.8 = (bf16[2048]{0:T(1024)(128)(2,1)S(1)}, bf16[2048]{0:T(1024)(128)(2,1)}, u32[]{:S(2)}) copy-start(bf16[2048]{0:T(1024)(128)(2,1)} %param.38) | copy-start | bytes 12292
  24.9 25.8 %copy-start.10 = (s32[24,2]{0,1:T(2,128)S(1)}, s32[24,2]{0,1:T(2,128)}, u32[]{:S(2)}) copy-start(s32[24,2]{0,1:T(2,128)} %param.43) | copy-start | bytes 580
  27.6 84.9 %all-gather.2.cloned.1.call-start = ((), (), s32[]{:S(2)}) async-start(), calls=%async_computation.6 | async-start | bytes 1671168 | tf_op jit(solution)/shard_map/all_gather | solution.py:130
  49.3 0.6 copy-start.4
  50.6 70.7 %reduce-scatter.3.cloned.1.call-start = ((), (), s32[]{:S(2)}) async-start(), calls=%async_computation.5 | async-start | bytes 589824 | tf_op jit(solution)/shard_map/reduce_scatter | solution.py:162
  79.2 2.2 copy-start.16
  86.4 143.8 %reduce-scatter.5.cloned.1.call-start = ((), (), s32[]{:S(2)}) async-start(), calls=%async_computation.7 | async-start | bytes 3244032 | tf_op jit(solution)/shard_map/reduce_scatter | solution.py:138
  112.6 3.2 %copy-start.17 = (bf16[2048,512]{1,0:T(8,128)(2,1)S(1)}, bf16[2048,512]{1,0:T(8,128)(2,1)}, u32[]{:S(2)}) copy-start(bf16[2048,512]{1,0:T(8,128)(2,1)} %param.41) | copy-start | bytes 6291460
  112.6 3.2 %copy-start.18 = (bf16[384,2048]{1,0:T(8,128)(2,1)S(1)}, bf16[384,2048]{1,0:T(8,128)(2,1)}, u32[]{:S(2)}) copy-start(bf16[384,2048]{1,0:T(8,128)(2,1)} %all-gather.2.cloned.1.call-done) | copy-start | bytes 4718596
  115.8 1.6 copy-start.3
  120.1 0.7 copy-start.9
  120.1 9.9 %copy-start.12 = (f32[64]{0:T(128)S(1)}, f32[64]{0:T(128)}, u32[]{:S(2)}) copy-start(f32[64]{0:T(128)} %copy-done.11) | copy-start | bytes 772
  120.1 9.9 %copy-start.14 = (f32[24,1]{0,1:T(1,128)S(1)}, f32[24,1]{0,1:T(1,128)}, u32[]{:S(2)}) copy-start(f32[24,1]{0,1:T(1,128)} %copy-done.13) | copy-start | bytes 292
  120.1 10.5 %copy-start.5 = (bf16[24,2048]{1,0:T(8,128)(2,1)S(1)}, bf16[24,2048]{1,0:T(8,128)(2,1)}, u32[]{:S(2)}) copy-start(bf16[24,2048]{1,0:T(8,128)(2,1)} %copy-done.4) | copy-start | bytes 294916
  120.1 21.0 %copy-start.15 = (f32[24,2]{0,1:T(2,128)S(1)}, f32[24,2]{0,1:T(2,128)}, u32[]{:S(2)}) copy-start(f32[24,2]{0,1:T(2,128)} %param.44) | copy-start | bytes 580
  123.1 17.1 %all-to-all-start.1 = ((bf16[16,6,1024]{2,1,0:T(8,128)(2,1)}), bf16[16,6,1024]{2,1,0:T(8,128)(2,1)S(1)}, u32[]{:S(2)}, u32[]{:S(2)}) async-start(bf16[16,6,1024]{2,1,0:T(8,128)(2,1)} %copy.67), calls=%async_computation.2 | async-start | bytes 524288 | tf_op jit(solution)/shard_map/all_to_all | solution.py:165
Sparse Core Ops, SparseCore 0:
  27.8 20.5 all-reduce.2
  51.1 61.4 all-gather.1
  114.8 6.5 reduce-scatter.2
  126.7 103.4 reduce-scatter.4
where the time goes:
time: 240 us; the launch traced here: 239 us
  waiting for transfers between devices  104 us (43%)
  blocking collectives  63.3 us (26%)
  matrix products  29.1 us (12%)
  between operations  14.2 us (6%)
  other arithmetic  12.2 us (5%)
  local copies, waits for them, and re-layouts  9.26 us (4%)
  starting transfers between devices  6.92 us (3%)
    reduce_scatter x1, waiting for transfers between devices, body(): lax.psum_scatter(dense_terms.reshape(-1, half_width), ('ep', 'tp'), scatt...  48.7 us
    unnamed x1, blocking collectives  38.9 us
    all_gather x1, waiting for transfers between devices, body(): all_tokens = lax.all_gather(post_norm, 'ep', axis=0, tiled=True)  26.2 us
    all_to_all x1, blocking collectives, body(): lax.all_to_all(outgoing, 'ep', split_axis=0, concat_axis=0, tiled=True)  24.4 us
    psum x1, waiting for transfers between devices, body(): lax.psum(partial_value.astype(jnp.bfloat16), 'tp').astype(jnp.float32)  20.6 us
    all_to_all x1, waiting for transfers between devices, body(): lax.all_to_all(halves, 'ep', split_axis=0, concat_axis=0, tiled=True)  7.95 us
    all_to_all x1, starting transfers between devices, body(): lax.all_to_all(halves, 'ep', split_axis=0, concat_axis=0, tiled=True)  6.76 us
    dot_general x2, matrix products, swiglu_rows(): jnp.dot(inputs, gate_weight, preferred_element_type=jnp.float32)  5.38 us
  transfers between devices with their start and end apart: 5, of which 5 were waited for; matrix products, arithmetic and copies ran while one was open for 10% of the time, Pallas kernels for 0%

commit v1 on v0

v1 whole, which is shorter than its diff:
```python
import functools
import jax
import jax.numpy as jnp
from jax import lax
from jax.experimental import pallas as pl
from jax.experimental.pallas import tpu as pltpu
from jax.sharding import PartitionSpec as P

FF2 = 16384
GROUPS = 4


norm_eps = 1e-06


def rms_scale(values, gain_vec):
    mean_square = jnp.mean(values * values, axis=-1, keepdims=True)
    return values * lax.rsqrt(mean_square + norm_eps) * gain_vec


MESH = pl.DeviceIdType.MESH


def fdot(a, b):
    return jnp.dot(a, b, preferred_element_type=jnp.float32)


def silu(v):
    return v / (1.0 + jnp.exp(-v))


def mlp_kernel(
    ep_count,
    zn,
    capp,
    ff2,
    heads_ref,
    tok_ref,
    gain_ref,
    gate_ref,
    place_ref,
    comb_ref,
    out_hbm,
    dg_hbm,
    du_hbm,
    dd_hbm,
    eg_hbm,
    eu_hbm,
    ed_hbm,
    res_ref,
    wout,
    wg,
    wu,
    wd_own,
    wd_oth,
    xg,
    xu,
    xd_own,
    xd_oth,
    part,
    part_in,
    resid,
    gath,
    hid,
    p_own,
    p_sq,
    p_send,
    p_recv,
    s_send,
    r_recv,
    t_send,
    z_recv,
    rows,
    act,
    e_own,
    e_send,
    e_recv,
    e_out,
    e_ret,
    wsem,
    tp_sem,
    a_send,
    a_recv,
    b_send,
    b_recv,
    f_send,
    f_recv,
    d_sem,
    rs_send,
    rs_recv,
    zs_send,
    zs_recv,
    x_sem,
    er_send,
    er_recv,
):
    pn = ep_count // zn
    me = lax.axis_index("ep")
    c = lax.axis_index("tp")
    z = me // pn
    q = me % pn
    other = 1 - c
    seq, width = tok_ref.shape
    half = width // 2
    full = gath.shape[2]
    fhalf = full // 2
    rows_all = ep_count * seq
    own_cols = pl.ds(pl.multiple_of(c * half, 128), half)
    oth_cols = pl.ds(pl.multiple_of(other * half, 128), half)
    g_cols = pl.ds(pl.multiple_of(c * fhalf, 128), fhalf)

    barrier = pltpu.get_barrier_semaphore()
    for d in range(1, ep_count):
        pl.semaphore_signal(
            barrier, inc=1, device_id=((me + d) % ep_count, c), device_id_type=MESH
        )
    pl.semaphore_signal(barrier, inc=1, device_id=(me, other), device_id_type=MESH)

    loads = [
        (out_hbm, wout),
        (dg_hbm, wg),
        (du_hbm, wu),
        (dd_hbm.at[:, oth_cols], wd_oth),
        (dd_hbm.at[:, own_cols], wd_own),
        (eg_hbm.at[0], xg),
        (eu_hbm.at[0], xu),
        (ed_hbm.at[0, :, oth_cols], xd_oth),
        (ed_hbm.at[0, :, own_cols], xd_own),
    ]
    loads = [pltpu.make_async_copy(a, b, wsem.at[i]) for i, (a, b) in enumerate(loads)]
    for one in loads:
        one.start()

    def remote(src, dst, ssem, rsem, ep_id, tp_id):
        return pltpu.make_async_remote_copy(
            src_ref=src,
            dst_ref=dst,
            send_sem=ssem,
            recv_sem=rsem,
            device_id=(ep_id, tp_id),
            device_id_type=MESH,
        )

    loads[0].wait()
    part[...] = fdot(heads_ref[...], wout[...]).astype(jnp.bfloat16)
    pl.semaphore_wait(barrier, ep_count)
    swap = remote(part, part_in, tp_sem.at[0], tp_sem.at[1], me, other)
    swap.start()
    swap.wait()
    attn = part[...].astype(jnp.float32) + part_in[...].astype(jnp.float32)
    res = (tok_ref[...].astype(jnp.float32) + attn).astype(jnp.bfloat16).astype(jnp.float32)
    resid[...] = res
    post = rms_scale(res, gain_ref[...].astype(jnp.float32)).astype(jnp.bfloat16)
    gath[me, :, :width] = post
    gath[me, :, width:] = place_ref[...]
    branch_in = jnp.sum(
        post.astype(jnp.float32) * gate_ref[...].astype(jnp.float32), axis=1, keepdims=True
    )
    branch = 1.0 / (1.0 + jnp.exp(-branch_in))

    sent = []

    def block_send(o, ssem, rsem, ep_id, tp_id):
        piece = gath.at[o, :, g_cols]
        one = remote(piece, piece, ssem, rsem, ep_id, tp_id)
        one.start()
        sent.append(one)
        return one

    z_sends = []
    for dz in range(1, zn):
        z_sends.append(
            block_send(me, a_send.at[dz], a_recv.at[dz], ((z + dz) % zn) * pn + q, c)
        )
    b_sends = {}
    f_sends = []

    def to_plane(o, dz):
        for dq in range(1, pn):
            b_sends[dz, dq] = block_send(
                o, b_send.at[dz, dq], b_recv.at[dz, dq], z * pn + (q + dq) % pn, c
            )

    to_plane(me, 0)
    for dz in range(1, zn):
        z_sends[dz - 1].wait_recv()
        o = ((z + zn - dz) % zn) * pn + q
        to_plane(o, dz)
        f_sends.append(block_send(o, f_send.at[dz, 0], f_recv.at[dz, 0], me, other))
    for dz in range(zn):
        for dq in range(1, pn):
            b_sends[dz, dq].wait_recv()
            o = ((z + zn - dz) % zn) * pn + (q + pn - dq) % pn
            f_sends.append(block_send(o, f_send.at[dz, dq], f_recv.at[dz, dq], me, other))
    for one in f_sends:
        one.wait_recv()
    for one in sent:
        one.wait_send()

    loads[1].wait()
    loads[2].wait()
    total_sq = jnp.zeros((rows_all, 1), jnp.float32)
    units = wg.shape[1]
    step = min(256, units)
    x = gath[:, :, :width].reshape(rows_all, width)
    for j in range(0, units, step):
        h = silu(fdot(x, wg[:, j : j + step])) * fdot(x, wu[:, j : j + step])
        total_sq = total_sq + jnp.sum(h * h, axis=1, keepdims=True)
        hid[:, j : j + step] = h.astype(jnp.bfloat16)
    lane_sq = jnp.broadcast_to(total_sq, (rows_all, 128)).reshape(ep_count, seq, 128)
    p_sq[...] = lane_sq
    p_send[:, :, half:] = lane_sq.astype(jnp.bfloat16)
    loads[3].wait()
    for j in range(0, half, step):
        term = fdot(hid[...], wd_oth[:, j : j + step])
        p_send[:, :, j : j + step] = term.astype(jnp.bfloat16).reshape(ep_count, seq, step)
    d_swap = remote(p_send, p_recv, d_sem.at[0], d_sem.at[1], me, other)
    d_swap.start()
    loads[4].wait()
    for j in range(0, half, step):
        p_own[:, :, j : j + step] = fdot(hid[...], wd_own[:, j : j + step]).reshape(
            ep_count, seq, step
        )
    d_swap.wait()

    def chip_sum(o):
        got = p_recv[o].astype(jnp.float32)
        return p_own[o] + got[:, :half], p_sq[o] + got[:, half:]

    plane_sends = {}
    for i in range(zn):
        dz = (i + 1) % zn
        for dq in range(1, pn):
            o = ((z + dz) % zn) * pn + (q + dq) % pn
            main, squares = chip_sum(o)
            s_send[o, :, :half] = main.astype(jnp.bfloat16)
            s_send[o, :, half:] = squares.astype(jnp.bfloat16)
            one = remote(
                s_send.at[o],
                r_recv.at[dq - 1, dz],
                rs_send.at[dz, dq],
                rs_recv.at[dz, dq],
                z * pn + (q + dq) % pn,
                c,
            )
            one.start()
            plane_sends[dz, dq] = one

    slots = ep_count * capp
    pick_from = lax.broadcasted_iota(jnp.int32, (full - width, slots), 0)
    pick_to = lax.broadcasted_iota(jnp.int32, (full - width, slots), 1) % capp
    pick = (pick_from == me * capp + pick_to).astype(jnp.float32).astype(jnp.bfloat16)
    chosen = fdot(gath[:, :, width:].reshape(rows_all, full - width), pick)
    row_owner = lax.broadcasted_iota(jnp.int32, (rows_all, slots), 0) // seq
    slot_owner = lax.broadcasted_iota(jnp.int32, (rows_all, slots), 1) // capp
    chosen = jnp.where(row_owner == slot_owner, chosen, 0.0).astype(jnp.bfloat16)
    for j in range(0, width, 512):
        rows[:, j : j + 512] = lax.dot_general(
            chosen,
            gath[:, :, j : j + 512].reshape(rows_all, 512),
            (((0,), (0,)), ((), ())),
            preferred_element_type=jnp.float32,
        ).astype(jnp.bfloat16)
    loads[5].wait()
    loads[6].wait()
    for j in range(0, xg.shape[1], step):
        act[:, j : j + step] = (
            silu(fdot(rows[...], xg[:, j : j + step])) * fdot(rows[...], xu[:, j : j + step])
        ).astype(jnp.bfloat16)
    loads[7].wait()
    for j in range(0, half, step):
        e_send[:, :, j : j + step] = (
            fdot(act[...], xd_oth[:, j : j + step])
            .reshape(ep_count, capp, step)
            .astype(jnp.bfloat16)
        )
    x_swap = remote(e_send, e_recv, x_sem.at[0], x_sem.at[1], me, other)
    x_swap.start()
    loads[8].wait()
    for j in range(0, half, step):
        e_own[:, :, j : j + step] = (
            fdot(act[...], xd_own[:, j : j + step])
            .reshape(ep_count, capp, step)
            .astype(jnp.bfloat16)
        )
    x_swap.wait()
    e_sum = (e_own[...].astype(jnp.float32) + e_recv[...].astype(jnp.float32)).astype(jnp.bfloat16)
    e_out[...] = e_sum
    e_ret[me] = e_out[me]
    backs = []
    for d in range(1, ep_count):
        peer = (me + d) % ep_count
        one = remote(e_out.at[peer], e_ret.at[me], er_send.at[d], er_recv.at[d], peer, c)
        one.start()
        backs.append(one)

    def plane_total(dz):
        main, squares = chip_sum(((z + dz) % zn) * pn + q)
        for dq in range(1, pn):
            plane_sends[dz, dq].wait_recv()
            got = r_recv[dq - 1, dz].astype(jnp.float32)
            main = main + got[:, :half]
            squares = squares + got[:, half:]
        return main, squares

    z_outs = []
    for dz in range(1, zn):
        main, squares = plane_total(dz)
        t_send[dz, :, :half] = main.astype(jnp.bfloat16)
        t_send[dz, :, half:] = squares.astype(jnp.bfloat16)
        one = remote(
            t_send.at[dz],
            z_recv.at[dz],
            zs_send.at[dz],
            zs_recv.at[dz],
            ((z + dz) % zn) * pn + q,
            c,
        )
        one.start()
        z_outs.append(one)
    main, squares = plane_total(0)
    for dz in range(1, zn):
        z_outs[dz - 1].wait_recv()
        got = z_recv[dz].astype(jnp.float32)
        main = main + got[:, :half]
        squares = squares + got[:, half:]
    inverse = lax.rsqrt(squares[:, :1] / ff2 + norm_eps)
    dense_out = (main * inverse).astype(jnp.bfloat16).astype(jnp.float32)
    for one in backs:
        one.wait_recv()
    returned = e_ret[...].reshape(slots, half)
    comb = comb_ref[...]
    comb_high = comb.astype(jnp.bfloat16)
    comb_low = (comb - comb_high.astype(jnp.float32)).astype(jnp.bfloat16)
    expert_sum = fdot(comb_high, returned) + fdot(comb_low, returned)
    res_ref[...] = (resid[:, own_cols] + expert_sum + branch * dense_out).astype(jnp.bfloat16)
    for one in plane_sends.values():
        one.wait_send()
    for one in z_outs:
        one.wait_send()
    for one in backs:
        one.wait_send()


def mlp_call(ep_count, capp, heads, tokens, gain, gate, place, comb, weights):
    zn = 2 ** ((ep_count.bit_length() - 1) // 2)
    pn = ep_count // zn
    seq, width = tokens.shape
    half = width // 2
    units = weights[1].shape[1]
    x_units = weights[4].shape[2]
    full = width + place.shape[1]
    slots = ep_count * capp
    lane = half + 128
    bf, f32 = jnp.bfloat16, jnp.float32
    dma = pltpu.SemaphoreType.DMA
    vm = pltpu.VMEM
    scratch = [
        vm(weights[0].shape, bf),
        vm((width, units), bf),
        vm((width, units), bf),
        vm((units, half), bf),
        vm((units, half), bf),
        vm((width, x_units), bf),
        vm((width, x_units), bf),
        vm((x_units, half), bf),
        vm((x_units, half), bf),
        vm((seq, width), bf),
        vm((seq, width), bf),
        vm((seq, width), f32),
        vm((ep_count, seq, full), bf),
        vm((ep_count * seq, units), bf),
        vm((ep_count, seq, half), f32),
        vm((ep_count, seq, 128), f32),
        vm((ep_count, seq, lane), bf),
        vm((ep_count, seq, lane), bf),
        vm((ep_count, seq, lane), bf),
        vm((pn - 1, zn, seq, lane), bf),
        vm((zn, seq, lane), bf),
        vm((zn, seq, lane), bf),
        vm((slots, width), bf),
        vm((slots, x_units), bf),
        vm((ep_count, capp, half), bf),
        vm((ep_count, capp, half), bf),
        vm((ep_count, capp, half), bf),
        vm((ep_count, capp, half), bf),
        vm((ep_count, capp, half), bf),
        dma((9,)),
        dma((2,)),
        dma((zn,)),
        dma((zn,)),
        dma((zn, pn)),
        dma((zn, pn)),
        dma((zn, pn)),
        dma((zn, pn)),
        dma((2,)),
        dma((zn, pn)),
        dma((zn, pn)),
        dma((zn,)),
        dma((zn,)),
        dma((2,)),
        dma((ep_count,)),
        dma((ep_count,)),
    ]
    return pl.pallas_call(
        functools.partial(mlp_kernel, ep_count, zn, capp, FF2),
        out_shape=jax.ShapeDtypeStruct((seq, half), bf),
        in_specs=[pl.BlockSpec(memory_space=pltpu.VMEM)] * 6
        + [pl.BlockSpec(memory_space=pl.ANY)] * 7,
        out_specs=pl.BlockSpec(memory_space=pltpu.VMEM),
        scratch_shapes=scratch,
        compiler_params=pltpu.CompilerParams(
            collective_id=0, has_side_effects=True, vmem_limit_bytes=60 * 1024 * 1024
        ),
    )(heads, tokens, gain, gate, place, comb, *weights)


def body(
    tokens,
    norm_gain,
    query_w,
    key_w,
    value_w,
    forget_w,
    forget_bias,
    query_gain,
    key_gain,
    cache_key,
    cache_value,
    cache_gate,
    cache_len,
    out_w,
    post_gain,
    branch_gate,
    dense_gate_w,
    dense_up_w,
    dense_down_w,
    expert_choice,
    route_weight,
    expert_gate_w,
    expert_up_w,
    expert_down_w,
):
    seq_count = tokens.shape[0]
    model_width = tokens.shape[1]
    heads_local = cache_gate.shape[1]
    kv_local = cache_key.shape[1]
    head_size = cache_key.shape[2]
    cache_span = cache_key.shape[3]
    tp_count = lax.axis_size("tp")
    ep_count = lax.axis_size("ep")
    tp_rank = lax.axis_index("tp")
    score_scale = head_size ** (-0.5)
    resid_in = tokens.astype(jnp.float32)
    normed = rms_scale(resid_in, norm_gain.astype(jnp.float32)).astype(jnp.bfloat16)
    queries = jnp.dot(normed, query_w, preferred_element_type=jnp.float32).reshape(
        seq_count, heads_local, head_size
    )
    queries = rms_scale(queries, query_gain.astype(jnp.float32)).astype(jnp.bfloat16)
    keys_all = jnp.dot(normed, key_w, preferred_element_type=jnp.float32).reshape(
        seq_count, -1, head_size
    )
    keys_all = rms_scale(keys_all, key_gain.astype(jnp.float32)).astype(jnp.bfloat16)
    values_all = (
        jnp.dot(normed, value_w, preferred_element_type=jnp.float32)
        .astype(jnp.bfloat16)
        .reshape(seq_count, -1, head_size)
    )
    fresh_key = lax.dynamic_slice_in_dim(keys_all, tp_rank * kv_local, kv_local, 1)
    fresh_value = lax.dynamic_slice_in_dim(values_all, tp_rank * kv_local, kv_local, 1)
    forget_all = jax.nn.log_sigmoid(
        jnp.dot(normed, forget_w, preferred_element_type=jnp.float32) + forget_bias
    )
    log_forget = lax.dynamic_slice_in_dim(forget_all, tp_rank * heads_local, heads_local, 1)
    repeat = heads_local // kv_local
    grouped = queries.reshape(seq_count, kv_local, repeat, head_size)
    scores = (
        jnp.einsum("sgrd,sgdl->sgrl", grouped, cache_key, preferred_element_type=jnp.float32)
        * score_scale
    )
    own_score = (
        jnp.einsum("sgrd,sgd->sgr", grouped, fresh_key, preferred_element_type=jnp.float32)
        * score_scale
    )
    current_slot_offset = lax.broadcasted_iota(jnp.int32, (seq_count, cache_span), 1)
    at_last = (current_slot_offset == cache_len[:, None] - 1)[:, None, :]
    previous = jnp.sum(jnp.where(at_last, cache_gate, jnp.zeros_like(cache_gate)), axis=2)
    current = previous + log_forget
    decay_bias = (current[:, :, None] - cache_gate).reshape(seq_count, kv_local, repeat, cache_span)
    is_valid = (current_slot_offset < cache_len[:, None])[:, None, None, :]
    logits = jnp.where(is_valid, scores + decay_bias, -jnp.inf)
    top_logit = jnp.maximum(jnp.max(logits, axis=3), own_score)
    weights = jnp.exp(logits - top_logit[..., None])
    own_weight = jnp.exp(own_score - top_logit)
    total_weight = jnp.sum(weights, axis=3) + own_weight
    cache_probs = (weights / total_weight[..., None]).astype(jnp.bfloat16)
    own_prob = (own_weight / total_weight).astype(jnp.bfloat16)
    mixed_heads = jnp.einsum(
        "sgrl,sgdl->sgrd", cache_probs, cache_value, preferred_element_type=jnp.float32
    )
    mixed_heads = (
        mixed_heads
        + own_prob.astype(jnp.float32)[..., None] * fresh_value.astype(jnp.float32)[:, :, None, :]
    )
    attn_heads = mixed_heads.reshape(seq_count, heads_local * head_size).astype(jnp.bfloat16)
    per_group = ep_count // GROUPS
    capacity = 2 * ((seq_count + 2 * per_group - 1) // (2 * per_group))
    capp = -(-capacity // 8) * 8
    route_count = expert_choice.shape[1]
    route_ids = expert_choice.reshape(-1)
    member = (route_ids[:, None] == jnp.arange(ep_count)[None, :]).astype(jnp.int32)
    slot_index = jnp.sum((jnp.cumsum(member, axis=0) - member) * member, axis=1)
    target = (route_ids * capp + slot_index).reshape(seq_count, route_count)
    slots = ep_count * capp
    place_width = -(-slots // 256) * 256
    hit = target[:, :, None] == jnp.arange(place_width)[None, None, :]
    place = jnp.any(hit, axis=1).astype(jnp.bfloat16)
    comb = jnp.sum(jnp.where(hit, route_weight[:, :, None], 0.0), axis=1)[:, :slots]
    mixed_out = mlp_call(
        ep_count,
        capp,
        attn_heads,
        tokens,
        post_gain.reshape(1, -1),
        branch_gate.reshape(1, -1),
        place,
        comb,
        (
            out_w,
            dense_gate_w,
            dense_up_w,
            dense_down_w,
            expert_gate_w,
            expert_up_w,
            expert_down_w,
        ),
    )
    return (mixed_out, fresh_key, fresh_value, current)


def solution(mesh):
    placed = (
        P("ep", None),
        P(),
        P(None, "tp"),
        P(),
        P(),
        P(),
        P(),
        P(),
        P(),
        P("ep", "tp", None, None),
        P("ep", "tp", None, None),
        P("ep", "tp", None),
        P("ep"),
        P("tp", None),
        P(),
        P(),
        P(None, ("ep", "tp")),
        P(None, ("ep", "tp")),
        P(("ep", "tp"), None),
        P("ep", None),
        P("ep", None),
        P("ep", None, "tp"),
        P("ep", None, "tp"),
        P("ep", "tp", None),
    )
    return jax.shard_map(
        body,
        mesh=mesh,
        in_specs=placed,
        out_specs=(P("ep", "tp"), P("ep", "tp", None), P("ep", "tp", None), P("ep", "tp")),
        check_vma=False,
    )
```

time: 240 us -> 69.9 us (0.29)
  waiting for transfers between devices: 104 us -> 0 us
  blocking collectives: 63.3 us -> 0 us
  Pallas kernels: 0 us -> 44.7 us
  matrix products: 29.1 us -> 10.8 us
  between operations: 14.2 us -> 0.89 us
  starting transfers between devices: 6.92 us -> 0 us
  local copies, waits for them, and re-layouts: 9.26 us -> 4.91 us
  other arithmetic: 12.2 us -> 8.18 us
    reduce_scatter x2 -> x0, waiting for transfers between devices: 49.4 us -> none  [the longest x1 48.7 us: body(): lax.psum_scatter(dense_terms.reshape(-1, half_width), ('ep', 'tp'), scatt...]
    pallas_call x0 -> x1, Pallas kernels: none -> 44.7 us  [mlp_call(): pl.pallas_call(functools.partial(mlp_kernel, ep_count, zn, capp, FF2), ou...]
    unnamed x1 -> x0, blocking collectives: 38.9 us -> none
    all_gather x1 -> x0, waiting for transfers between devices: 26.2 us -> none  [body(): all_tokens = lax.all_gather(post_norm, 'ep', axis=0, tiled=True)]
    all_to_all x1 -> x0, blocking collectives: 24.4 us -> none  [body(): lax.all_to_all(outgoing, 'ep', split_axis=0, concat_axis=0, tiled=True)]
    psum x1 -> x0, waiting for transfers between devices: 20.6 us -> none  [body(): lax.psum(partial_value.astype(jnp.bfloat16), 'tp').astype(jnp.float32)]
    dot_general x10 -> x0, matrix products: 19.1 us -> none  [the longest x2 5.38 us: swiglu_rows(): jnp.dot(inputs, gate_weight, preferred_element_type=jnp.float32)]
    all_to_all x1 -> x0, waiting for transfers between devices: 7.95 us -> none  [body(): lax.all_to_all(halves, 'ep', split_axis=0, concat_axis=0, tiled=True)]
  transfers between devices with their start and end apart: 5 -> 0, of which waited for: 5 -> 0; matrix products, arithmetic and copies ran while one was open for 10% -> 0% of each run, Pallas kernels for 0% -> 0%
where the time goes in v1:
time: 69.9 us; the launch traced here: 69.4 us
  Pallas kernels  44.7 us (64%)
  matrix products  10.8 us (15%)
  other arithmetic  8.18 us (12%)
  local copies, waits for them, and re-layouts  4.91 us (7%)
  between operations  0.89 us (1%)
    pallas_call x1, Pallas kernels, mlp_call(): pl.pallas_call(functools.partial(mlp_kernel, ep_count, zn, capp, FF2), ou...  44.7 us
    dot_general x1, matrix products, body(): jnp.einsum('sgrl,sgdl->sgrd', cache_probs, cache_value, preferred_element...  3.15 us
    dot_general x1, matrix products, body(): jnp.einsum('sgrd,sgdl->sgrl', grouped, cache_key, preferred_element_type=...  2.66 us
    dot_general x1, matrix products, body(): jnp.dot(normed, query_w, preferred_element_type=jnp.float32)  2.07 us
    unnamed x24, local copies, waits for them, and re-layouts  1.56 us

profile of v1, /device:TPU:0, one launch (start us, length us, event | category | flops | bytes accessed | tf_op | source)
XLA Modules:
  0.0 69.4 jit_solution(11362426536292312941)
XLA Ops:
  0.7 0.8 %broadcast_add_fusion = s32[24]{0:T(128)S(1)} fusion(s32[24]{0:T(128)} %param.36), kind=kLoop, calls=%fused_computation.59 | loop fusion | flops 24 | bytes 192 | tf_op jit(solution)/shard_map/sub | solution.py:486
  1.5 0.1 iota_compare_fusion
  1.6 1.4 %select_reduce_fusion = f32[24,8]{1,0:T(8,128)S(1)} fusion(f32[24,8,1024]{2,1,0:T(8,128)} %param.35, pred[24,1024]{1,0:T(8,128)(4,1)S(1)} %iota_compare_fusion), kind=kLoop, calls=%fused_computation.14 | loop fusion | flops 393024 | bytes 811776 | tf_op jit(solution)/shard_map/reduce_sum | solution.py:487
  3.0 0.7 convert_element_type.52
  3.7 1.0 %fusion.23 = f32[24]{0:T(128)S(1)} fusion(bf16[24,2048]{1,0:T(8,128)(2,1)} %tok_ref.1), kind=kLoop, calls=%fused_computation.20 | loop fusion | flops 147432 | bytes 98400 | tf_op jit(solution)/shard_map/reduce_sum | solution.py:17
  4.7 1.2 %fusion.45 = (f32[24,16]{0,1:T(8,128)S(1)}, f32[24,16]{0,1:T(8,128)S(1)}) fusion(f32[16]{0:T(128)} %param.30, bf16[2048,16]{0,1:T(8,128)(2,1)} %param.29, bf16[24,2048]{1,0:T(8,128)(2,1)} %tok_ref.1, f32[2048]{0:T(1024)S(1)} %convert_element_type.52, f32[24]{0:T(128)S(1)} %add_rsqrt_fusion.2), kind=kOutput, calls=%fused_computation.62 | convolution fusion | flops 1770624 | bytes 175264 | tf_op jit(solution)/shard_map/dot_general | solution.py:472
  6.0 2.1 %fusion.43 = f32[24,512]{1,0:T(8,128)S(1)} fusion(bf16[2048,512]{1,0:T(8,128)(2,1)} %param.26, bf16[24,2048]{1,0:T(8,128)(2,1)} %tok_ref.1, f32[2048]{0:T(1024)S(1)} %convert_element_type.52, f32[24]{0:T(128)S(1)} %add_rsqrt_fusion.2), kind=kOutput, calls=%fused_computation.61 | convolution fusion | flops 50528256 | bytes 2252896 | tf_op jit(solution)/shard_map/dot_general | solution.py:456
  8.1 0.1 reshape.157
  8.2 0.1 multiply_reduce_fusion
  8.3 0.1 iota_compare_fusion.1
  8.5 2.7 %fusion.46 = (f32[24,8]{1,0:T(8,128)S(1)}, f32[24,8,1024]{2,1,0:T(8,128)}) fusion(f32[24,8,1024]{2,1,0:T(8,128)} %param.35, f32[24,8]{1,0:T(8,128)S(1)} %copy.61, bf16[24,1,64,1024]{3,2,1,0:T(8,128)(2,1)S(1)} %copy-done, f32[24,8,64]{2,1,0:T(8,128)S(1)} %reshape.157, f32[64]{0:T(128)S(1)} %convert_element_type.54, f32[24,8]{1,0:T(8,128)S(1)} %add_rsqrt_fusion, ...), kind=kOutput, calls=%fused_computation.63 | convolution fusion | flops 26185536 | bytes 4794880 | tf_op jit(solution)/shard_map/sgrd,sgdl->sgrl/dot_general | solution.py:478
  11.2 0.2 fusion.40
  11.4 0.1 reshape.159
  11.5 0.1 multiply_reduce_fusion.1
  11.8 0.2 fusion.30
  12.1 1.4 %fusion.20 = f32[24,8]{1,0:T(8,128)S(1)} fusion(f32[24,8,1024]{2,1,0:T(8,128)} %get-tuple-element.11, f32[24,8]{1,0:T(8,128)S(1)} %multiply_maximum_fusion), kind=kLoop, calls=%fused_computation.15 | loop fusion | flops 393024 | bytes 787968 | tf_op jit(solution)/shard_map/reduce_sum | solution.py:495
  13.5 1.3 %convolution_convert_fusion = bf16[24,128]{1,0:T(8,128)(2,1)S(1)} fusion(bf16[2048,128]{1,0:T(8,128)(2,1)} %param.28, bf16[24,2048]{1,0:T(8,128)(2,1)S(1)} %copy-done.1, f32[2048]{0:T(1024)S(1)} %convert_element_type.52, f32[24]{0:T(128)S(1)} %add_rsqrt_fusion.2), kind=kOutput, calls=%fused_computation.9 | convolution fusion | flops 12782592 | bytes 637024 | tf_op jit(solution)/shard_map/dot_general | solution.py:465
  14.8 0.1 reshape.162
  14.9 0.6 bitcast_convert_fusion
  15.5 3.2 %fusion.16 = bf16[24,8,64]{2,1,0:T(8,128)(2,1)S(1)} fusion(bf16[24,1,64,1024]{3,2,1,0:T(8,128)(2,1)} %param.34, f32[24,8,1024]{2,1,0:T(8,128)} %get-tuple-element.11, f32[24,8]{1,0:T(8,128)S(1)} %get-tuple-element.7, f32[24,8]{1,0:T(8,128)S(1)} %multiply_maximum_fusion, f32[24,64]{1,0:T(8,128)S(1)} %get-tuple-element.4, f32[24,8]{1,0:T(8,128)S(1)} %get-tuple-element.6), kind=kOutput, calls=%fused_computation.8 | convolution fusion | flops 25792512 | bytes 3965184 | tf_op jit(solution)/shard_map/sgrl,sgdl->sgrd/dot_general | solution.py:498
  18.6 0.7 %convert_element_type.63.heads_ref = bf16[24,512]{1,0:T(8,128)(2,1)} reshape(bf16[24,8,64]{2,1,0:T(8,128)(2,1)S(1)} %fusion.16) | data formatting | bytes 49152 | tf_op jit(solution)/shard_map/convert_element_type | solution.py:505
  19.4 0.6 reshape.163.gain_ref
  20.0 0.6 reshape.164.gate_ref
  20.6 0.1 copy.65
  20.7 0.1 eq.42
  20.9 0.2 select_reduce_fusion.2
  21.1 0.1 reduce_sum.71
  21.4 0.6 convert_element_type.65.place_ref
  22.1 0.6 slice.4.comb_ref
  22.7 44.7 %shard_map.255 = bf16[24,1024]{1,0:T(8,128)(2,1)} custom-call(bf16[24,512]{1,0:T(8,128)(2,1)} %convert_element_type.63.heads_ref, bf16[24,2048]{1,0:T(8,128)(2,1)} %tok_ref.1, bf16[1,2048]{1,0:T(2,128)(2,1)} %reshape.163.gain_ref, bf16[1,2048]{1,0:T(2,128)(2,1)} %reshape.164.gate_ref, bf16[24,256]{1,0:T(8,128)(2,1)} %convert_element_type.65.place_ref, ...), custom_call_target="tpu_custom_call" | custom-call | tf_op jit(solution)/shard_map/pallas_call | solution.py:405
  67.4 0.7 fusion.29
  68.0 1.4 %copy.82 = bf16[24,1024]{1,0:T(8,128)(2,1)} copy(bf16[24,1024]{1,0:T(8,128)(2,1)} %shard_map.255) | data formatting | bytes 98304
  (43 shorter events, 0.9 us)
Async XLA Ops:
  0.6 7.8 %copy-start = (bf16[24,1,64,1024]{3,2,1,0:T(8,128)(2,1)S(1)}, bf16[24,1,64,1024]{3,2,1,0:T(8,128)(2,1)}, u32[]{:S(2)}) copy-start(bf16[24,1,64,1024]{3,2,1,0:T(8,128)(2,1)} %param.33) | copy-start | bytes 9437188
  0.6 7.7 %copy-start.8 = (s32[24]{0:T(128)S(1)}, s32[24]{0:T(128)}, u32[]{:S(2)}) copy-start(s32[24]{0:T(128)} %param.36) | copy-start | bytes 292
  0.7 7.5 %copy-start.9 = (bf16[64]{0:T(256)(128)(2,1)S(1)}, bf16[64]{0:T(256)(128)(2,1)}, u32[]{:S(2)}) copy-start(bf16[64]{0:T(256)(128)(2,1)} %param.31) | copy-start | bytes 388
  5.9 5.2 %copy-start.3 = (f32[24,8]{0,1:T(8,128)}, f32[24,8]{0,1:T(8,128)S(1)}, u32[]{:S(2)}) copy-start(f32[24,8]{0,1:T(8,128)S(1)} %fusion.34) | copy-start | bytes 2308
  8.4 2.7 %copy-start.10 = (bf16[64]{0:T(256)(128)(2,1)S(1)}, bf16[64]{0:T(256)(128)(2,1)}, u32[]{:S(2)}) copy-start(bf16[64]{0:T(256)(128)(2,1)} %param.32) | copy-start | bytes 388
  8.5 2.7 %copy-start.1 = (bf16[24,2048]{1,0:T(8,128)(2,1)S(1)}, bf16[24,2048]{1,0:T(8,128)(2,1)}, u32[]{:S(2)}) copy-start(bf16[24,2048]{1,0:T(8,128)(2,1)} %tok_ref.1) | copy-start | bytes 294916
  8.5 2.7 %copy-start.2 = (bf16[2048,128]{1,0:T(8,128)(2,1)S(1)}, bf16[2048,128]{1,0:T(8,128)(2,1)}, u32[]{:S(2)}) copy-start(bf16[2048,128]{1,0:T(8,128)(2,1)} %param.27) | copy-start | bytes 1572868
  15.5 3.9 %copy-start.4 = (bf16[2048]{0:T(1024)(128)(2,1)S(1)}, bf16[2048]{0:T(1024)(128)(2,1)}, u32[]{:S(2)}) copy-start(bf16[2048]{0:T(1024)(128)(2,1)} %param.38) | copy-start | bytes 12292
  15.5 4.5 %copy-start.5 = (bf16[2048]{0:T(1024)(128)(2,1)S(1)}, bf16[2048]{0:T(1024)(128)(2,1)}, u32[]{:S(2)}) copy-start(bf16[2048]{0:T(1024)(128)(2,1)} %param.39) | copy-start | bytes 12292
  15.5 5.1 %copy-start.6 = (s32[24,2]{0,1:T(2,128)S(1)}, s32[24,2]{0,1:T(2,128)}, u32[]{:S(2)}) copy-start(s32[24,2]{0,1:T(2,128)} %param.43) | copy-start | bytes 580
  15.5 6.5 %copy-start.7 = (f32[24,2]{0,1:T(2,128)S(1)}, f32[24,2]{0,1:T(2,128)}, u32[]{:S(2)}) copy-start(f32[24,2]{0,1:T(2,128)} %param.44) | copy-start | bytes 580

commit v2 on v1

--- a/solution.py
+++ b/solution.py
@@ -38,8 +38,8 @@
     tok_ref,
     gain_ref,
     gate_ref,
-    place_ref,
-    comb_ref,
+    choice_ref,
+    weight_ref,
     out_hbm,
     dg_hbm,
     du_hbm,
@@ -141,6 +141,20 @@
             device_id_type=MESH,
         )
 
+    slots = ep_count * capp
+    lanes = full - width
+    lane_id = lax.broadcasted_iota(jnp.int32, (seq, lanes), 1)
+    first = choice_ref[:, 0:1] == lane_id // capp
+    second = choice_ref[:, 1:2] == lane_id // capp
+    named = jnp.where(first, 1.0, jnp.where(second, 1.0, 0.0))
+    earlier = lax.broadcasted_iota(jnp.int32, (seq, seq), 1) < lax.broadcasted_iota(
+        jnp.int32, (seq, seq), 0
+    )
+    earlier = jnp.where(earlier, 1.0, 0.0).astype(jnp.bfloat16)
+    rank = fdot(earlier, named.astype(jnp.bfloat16))
+    hit = jnp.where(rank == (lane_id % capp).astype(jnp.float32), named, 0.0)
+    comb = hit * jnp.where(first, weight_ref[:, 0:1], weight_ref[:, 1:2])
+    gath[me, :, width:] = hit.astype(jnp.bfloat16)
     loads[0].wait()
     part[...] = fdot(heads_ref[...], wout[...]).astype(jnp.bfloat16)
     pl.semaphore_wait(barrier, ep_count)
@@ -152,7 +166,6 @@
     resid[...] = res
     post = rms_scale(res, gain_ref[...].astype(jnp.float32)).astype(jnp.bfloat16)
     gath[me, :, :width] = post
-    gath[me, :, width:] = place_ref[...]
     branch_in = jnp.sum(
         post.astype(jnp.float32) * gate_ref[...].astype(jnp.float32), axis=1, keepdims=True
     )
@@ -173,7 +186,7 @@
             block_send(me, a_send.at[dz], a_recv.at[dz], ((z + dz) % zn) * pn + q, c)
         )
     b_sends = {}
-    f_sends = []
+    f_sends = {}
 
     def to_plane(o, dz):
         for dq in range(1, pn):
@@ -181,35 +194,48 @@
                 o, b_send.at[dz, dq], b_recv.at[dz, dq], z * pn + (q + dq) % pn, c
             )
 
+    def to_partner(o, dz, dq):
+        f_sends[dz, dq] = block_send(o, f_send.at[dz, dq], f_recv.at[dz, dq], me, other)
+
+    units = wg.shape[1]
+    step = min(256, units)
+    group_rows = pn * seq
+
+    def hidden_rows(dz):
+        for dq in range(pn):
+            if (dz, dq) in f_sends:
+                f_sends[dz, dq].wait_recv()
+        base = ((z + zn - dz) % zn) * pn
+        blocks = pl.ds(base, pn)
+        at_rows = pl.ds(pl.multiple_of(base * seq, group_rows), group_rows)
+        x = gath[blocks, :, :width].reshape(group_rows, width)
+        total_sq = jnp.zeros((group_rows, 1), jnp.float32)
+        for j in range(0, units, step):
+            h = silu(fdot(x, wg[:, j : j + step])) * fdot(x, wu[:, j : j + step])
+            total_sq = total_sq + jnp.sum(h * h, axis=1, keepdims=True)
+            hid[at_rows, j : j + step] = h.astype(jnp.bfloat16)
+        lane_sq = jnp.broadcast_to(total_sq, (group_rows, 128)).reshape(pn, seq, 128)
+        p_sq[blocks] = lane_sq
+        p_send[blocks, :, half:] = lane_sq.astype(jnp.bfloat16)
+
     to_plane(me, 0)
     for dz in range(1, zn):
         z_sends[dz - 1].wait_recv()
         o = ((z + zn - dz) % zn) * pn + q
         to_plane(o, dz)
-        f_sends.append(block_send(o, f_send.at[dz, 0], f_recv.at[dz, 0], me, other))
+        to_partner(o, dz, 0)
+    loads[1].wait()
+    loads[2].wait()
     for dz in range(zn):
         for dq in range(1, pn):
             b_sends[dz, dq].wait_recv()
             o = ((z + zn - dz) % zn) * pn + (q + pn - dq) % pn
-            f_sends.append(block_send(o, f_send.at[dz, dq], f_recv.at[dz, dq], me, other))
-    for one in f_sends:
-        one.wait_recv()
+            to_partner(o, dz, dq)
+        if dz > 0:
+            hidden_rows(dz - 1)
+    hidden_rows(zn - 1)
     for one in sent:
         one.wait_send()
-
-    loads[1].wait()
-    loads[2].wait()
-    total_sq = jnp.zeros((rows_all, 1), jnp.float32)
-    units = wg.shape[1]
-    step = min(256, units)
-    x = gath[:, :, :width].reshape(rows_all, width)
-    for j in range(0, units, step):
-        h = silu(fdot(x, wg[:, j : j + step])) * fdot(x, wu[:, j : j + step])
-        total_sq = total_sq + jnp.sum(h * h, axis=1, keepdims=True)
-        hid[:, j : j + step] = h.astype(jnp.bfloat16)
-    lane_sq = jnp.broadcast_to(total_sq, (rows_all, 128)).reshape(ep_count, seq, 128)
-    p_sq[...] = lane_sq
-    p_send[:, :, half:] = lane_sq.astype(jnp.bfloat16)
     loads[3].wait()
     for j in range(0, half, step):
         term = fdot(hid[...], wd_oth[:, j : j + step])
@@ -246,7 +272,6 @@
             one.start()
             plane_sends[dz, dq] = one
 
-    slots = ep_count * capp
     pick_from = lax.broadcasted_iota(jnp.int32, (full - width, slots), 0)
     pick_to = lax.broadcasted_iota(jnp.int32, (full - width, slots), 1) % capp
     pick = (pick_from == me * capp + pick_to).astype(jnp.float32).astype(jnp.bfloat16)
@@ -329,7 +354,7 @@
     for one in backs:
         one.wait_recv()
     returned = e_ret[...].reshape(slots, half)
-    comb = comb_ref[...]
+    comb = comb[:, :slots]
     comb_high = comb.astype(jnp.bfloat16)
     comb_low = (comb - comb_high.astype(jnp.float32)).astype(jnp.bfloat16)
     expert_sum = fdot(comb_high, returned) + fdot(comb_low, returned)
@@ -342,15 +367,15 @@
         one.wait_send()
 
 
-def mlp_call(ep_count, capp, heads, tokens, gain, gate, place, comb, weights):
+def mlp_call(ep_count, capp, heads, tokens, gain, gate, choice, route_weight, weights):
     zn = 2 ** ((ep_count.bit_length() - 1) // 2)
     pn = ep_count // zn
     seq, width = tokens.shape
     half = width // 2
     units = weights[1].shape[1]
     x_units = weights[4].shape[2]
-    full = width + place.shape[1]
     slots = ep_count * capp
+    full = width - (-slots // 256) * 256
     lane = half + 128
     bf, f32 = jnp.bfloat16, jnp.float32
     dma = pltpu.SemaphoreType.DMA
@@ -412,7 +437,7 @@
         compiler_params=pltpu.CompilerParams(
             collective_id=0, has_side_effects=True, vmem_limit_bytes=60 * 1024 * 1024
         ),
-    )(heads, tokens, gain, gate, place, comb, *weights)
+    )(heads, tokens, gain, gate, choice, route_weight, *weights)
 
 
 def body(
@@ -506,16 +531,6 @@
     per_group = ep_count // GROUPS
     capacity = 2 * ((seq_count + 2 * per_group - 1) // (2 * per_group))
     capp = -(-capacity // 8) * 8
-    route_count = expert_choice.shape[1]
-    route_ids = expert_choice.reshape(-1)
-    member = (route_ids[:, None] == jnp.arange(ep_count)[None, :]).astype(jnp.int32)
-    slot_index = jnp.sum((jnp.cumsum(member, axis=0) - member) * member, axis=1)
-    target = (route_ids * capp + slot_index).reshape(seq_count, route_count)
-    slots = ep_count * capp
-    place_width = -(-slots // 256) * 256
-    hit = target[:, :, None] == jnp.arange(place_width)[None, None, :]
-    place = jnp.any(hit, axis=1).astype(jnp.bfloat16)
-    comb = jnp.sum(jnp.where(hit, route_weight[:, :, None], 0.0), axis=1)[:, :slots]
     mixed_out = mlp_call(
         ep_count,
         capp,
@@ -523,8 +538,8 @@
         tokens,
         post_gain.reshape(1, -1),
         branch_gate.reshape(1, -1),
-        place,
-        comb,
+        expert_choice,
+        route_weight,
         (
             out_w,
             dense_gate_w,

time: 69.9 us -> 68.1 us (0.974)
  other arithmetic: 8.18 us -> 7.07 us
  Pallas kernels: 44.7 us -> 43.6 us
    unnamed x24 -> x25, local copies, waits for them, and re-layouts: 1.56 us -> 2.84 us
    pallas_call x1, Pallas kernels: 44.7 us -> 43.6 us  [mlp_call(): pl.pallas_call(functools.partial(mlp_kernel, ep_count, zn, capp, FF2), ou...]
where the time goes in v2:
time: 68.1 us; the launch traced here: 67.6 us
  Pallas kernels  43.6 us (64%)
  matrix products  10.8 us (16%)
  other arithmetic  7.07 us (10%)
  local copies, waits for them, and re-layouts  5.3 us (8%)
  between operations  0.87 us (1%)
    pallas_call x1, Pallas kernels, mlp_call(): pl.pallas_call(functools.partial(mlp_kernel, ep_count, zn, capp, FF2), ou...  43.6 us
    dot_general x1, matrix products, body(): jnp.einsum('sgrl,sgdl->sgrd', cache_probs, cache_value, preferred_element...  3.15 us
    unnamed x25, local copies, waits for them, and re-layouts  2.84 us
    dot_general x1, matrix products, body(): jnp.einsum('sgrd,sgdl->sgrl', grouped, cache_key, preferred_element_type=...  2.66 us
    dot_general x1, matrix products, body(): jnp.dot(normed, query_w, preferred_element_type=jnp.float32)  2.07 us
    reduce_sum x1, other arithmetic, body(): total_weight = jnp.sum(weights, axis=3) + own_weight  1.39 us
    reduce_sum x1, other arithmetic, body(): jnp.sum(jnp.where(at_last, cache_gate, jnp.zeros_like(cache_gate)), axis=2)  1.38 us

profile of v2, /device:TPU:0, one launch (start us, length us, event | category | flops | bytes accessed | tf_op | source)
XLA Modules:
  0.0 67.6 jit_solution(2385097190249427153)
XLA Ops:
  0.7 0.8 %broadcast_add_fusion = s32[24]{0:T(128)S(1)} fusion(s32[24]{0:T(128)} %param.36), kind=kLoop, calls=%fused_computation.52 | loop fusion | flops 24 | bytes 192 | tf_op jit(solution)/shard_map/sub | solution.py:511
  1.5 0.1 iota_compare_fusion
  1.6 1.4 %select_reduce_fusion = f32[24,8]{1,0:T(8,128)S(1)} fusion(f32[24,8,1024]{2,1,0:T(8,128)} %param.35, pred[24,1024]{1,0:T(8,128)(4,1)S(1)} %iota_compare_fusion), kind=kLoop, calls=%fused_computation.14 | loop fusion | flops 393024 | bytes 811776 | tf_op jit(solution)/shard_map/reduce_sum | solution.py:512
  3.0 0.1 copy.40
  3.0 0.7 %convert_element_type.46 = f32[2048]{0:T(1024)S(1)} convert(bf16[2048]{0:T(1024)(128)(2,1)} %param.25) | non-fusion elementwise | flops 2048 | bytes 12288 | tf_op jit(solution)/shard_map/convert_element_type | solution.py:480
  3.7 1.0 %fusion.23 = f32[24]{0:T(128)S(1)} fusion(bf16[24,2048]{1,0:T(8,128)(2,1)} %tok_ref.1), kind=kLoop, calls=%fused_computation.20 | loop fusion | flops 147432 | bytes 98400 | tf_op jit(solution)/shard_map/reduce_sum | solution.py:17
  4.7 1.2 %fusion.43 = (f32[24,16]{0,1:T(8,128)S(1)}, f32[24,16]{0,1:T(8,128)S(1)}) fusion(f32[16]{0:T(128)} %param.30, bf16[2048,16]{0,1:T(8,128)(2,1)} %param.29, bf16[24,2048]{1,0:T(8,128)(2,1)} %tok_ref.1, f32[2048]{0:T(1024)S(1)} %convert_element_type.46, f32[24]{0:T(128)S(1)} %add_rsqrt_fusion.2), kind=kOutput, calls=%fused_computation.55 | convolution fusion | flops 1770624 | bytes 175264 | tf_op jit(solution)/shard_map/dot_general | solution.py:497
  6.0 0.1 copy.41
  6.0 2.1 %fusion.41 = f32[24,512]{1,0:T(8,128)S(1)} fusion(bf16[2048,512]{1,0:T(8,128)(2,1)} %param.26, bf16[24,2048]{1,0:T(8,128)(2,1)} %tok_ref.1, f32[2048]{0:T(1024)S(1)} %convert_element_type.46, f32[24]{0:T(128)S(1)} %add_rsqrt_fusion.2), kind=kOutput, calls=%fused_computation.54 | convolution fusion | flops 50528256 | bytes 2252896 | tf_op jit(solution)/shard_map/dot_general | solution.py:481
  8.1 0.1 reshape.148
  8.2 0.1 multiply_reduce_fusion
  8.3 0.1 iota_compare_fusion.1
  8.5 2.7 %fusion.44 = (f32[24,8]{1,0:T(8,128)S(1)}, f32[24,8,1024]{2,1,0:T(8,128)}) fusion(f32[24,8,1024]{2,1,0:T(8,128)} %param.35, f32[24,8]{1,0:T(8,128)S(1)} %copy.41, bf16[24,1,64,1024]{3,2,1,0:T(8,128)(2,1)S(1)} %copy-done, f32[24,8,64]{2,1,0:T(8,128)S(1)} %reshape.148, f32[64]{0:T(128)S(1)} %convert_element_type.48, f32[24,8]{1,0:T(8,128)S(1)} %add_rsqrt_fusion, ...), kind=kOutput, calls=%fused_computation.56 | convolution fusion | flops 26185536 | bytes 4794880 | tf_op jit(solution)/shard_map/sgrd,sgdl->sgrl/dot_general | solution.py:503
  11.2 0.2 fusion.38
  11.4 0.1 reshape.150
  11.5 0.1 multiply_reduce_fusion.1
  11.6 0.1 copy.42
  11.7 0.1 fusion.49
  11.8 0.2 fusion.28
  12.1 1.4 %fusion.20 = f32[24,8]{1,0:T(8,128)S(1)} fusion(f32[24,8,1024]{2,1,0:T(8,128)} %get-tuple-element.11, f32[24,8]{1,0:T(8,128)S(1)} %multiply_maximum_fusion), kind=kLoop, calls=%fused_computation.15 | loop fusion | flops 393024 | bytes 787968 | tf_op jit(solution)/shard_map/reduce_sum | solution.py:520
  13.5 1.3 %convolution_convert_fusion = bf16[24,128]{1,0:T(8,128)(2,1)S(1)} fusion(bf16[2048,128]{1,0:T(8,128)(2,1)} %param.28, bf16[24,2048]{1,0:T(8,128)(2,1)S(1)} %copy-done.1, f32[2048]{0:T(1024)S(1)} %convert_element_type.46, f32[24]{0:T(128)S(1)} %add_rsqrt_fusion.2), kind=kOutput, calls=%fused_computation.9 | convolution fusion | flops 12782592 | bytes 637024 | tf_op jit(solution)/shard_map/dot_general | solution.py:490
  14.8 0.1 reshape.153
  14.9 0.6 bitcast_convert_fusion
  15.5 3.2 %fusion.16 = bf16[24,8,64]{2,1,0:T(8,128)(2,1)S(1)} fusion(bf16[24,1,64,1024]{3,2,1,0:T(8,128)(2,1)} %param.34, f32[24,8,1024]{2,1,0:T(8,128)} %get-tuple-element.11, f32[24,8]{1,0:T(8,128)S(1)} %get-tuple-element.7, f32[24,8]{1,0:T(8,128)S(1)} %multiply_maximum_fusion, f32[24,64]{1,0:T(8,128)S(1)} %get-tuple-element.4, f32[24,8]{1,0:T(8,128)S(1)} %get-tuple-element.6), kind=kOutput, calls=%fused_computation.8 | convolution fusion | flops 25792512 | bytes 3965184 | tf_op jit(solution)/shard_map/sgrl,sgdl->sgrd/dot_general | solution.py:523
  18.6 0.7 %convert_element_type.57.heads_ref = bf16[24,512]{1,0:T(8,128)(2,1)} reshape(bf16[24,8,64]{2,1,0:T(8,128)(2,1)S(1)} %fusion.16) | data formatting | bytes 49152 | tf_op jit(solution)/shard_map/convert_element_type | solution.py:530
  19.4 0.6 reshape.154.gain_ref
  20.0 0.6 reshape.155.gate_ref
  20.6 0.7 %copy.45.choice_ref = s32[24,2]{1,0:T(8,128)} copy(s32[24,2]{0,1:T(2,128)S(1)} %copy-done.6) | data formatting | bytes 384 | tf_op args[19]
  21.3 0.7 %copy.46.weight_ref = f32[24,2]{1,0:T(8,128)} copy(f32[24,2]{0,1:T(2,128)S(1)} %copy-done.7) | data formatting | bytes 384 | tf_op args[20]
  21.9 43.6 %shard_map.255 = bf16[24,1024]{1,0:T(8,128)(2,1)} custom-call(bf16[24,512]{1,0:T(8,128)(2,1)} %convert_element_type.57.heads_ref, bf16[24,2048]{1,0:T(8,128)(2,1)} %tok_ref.1, bf16[1,2048]{1,0:T(2,128)(2,1)} %reshape.154.gain_ref, bf16[1,2048]{1,0:T(2,128)(2,1)} %reshape.155.gate_ref, s32[24,2]{1,0:T(8,128)} %copy.45.choice_ref, f32[24,2]{1,0:T(8,128)} %copy.46.weight_ref, ...), custom_call_target="tpu_custom_call" | custom-call | tf_op jit(solution)/shard_map/pallas_call | solution.py:430
  65.5 0.7 fusion.27
  66.2 1.4 %copy.62 = bf16[24,1024]{1,0:T(8,128)(2,1)} copy(bf16[24,1024]{1,0:T(8,128)(2,1)} %shard_map.255) | data formatting | bytes 98304
  (33 shorter events, 0.2 us)
Async XLA Ops:
  0.6 7.8 %copy-start = (bf16[24,1,64,1024]{3,2,1,0:T(8,128)(2,1)S(1)}, bf16[24,1,64,1024]{3,2,1,0:T(8,128)(2,1)}, u32[]{:S(2)}) copy-start(bf16[24,1,64,1024]{3,2,1,0:T(8,128)(2,1)} %param.33) | copy-start | bytes 9437188
  0.6 7.7 %copy-start.8 = (s32[24]{0:T(128)S(1)}, s32[24]{0:T(128)}, u32[]{:S(2)}) copy-start(s32[24]{0:T(128)} %param.36) | copy-start | bytes 292
  0.7 7.5 %copy-start.9 = (bf16[64]{0:T(256)(128)(2,1)S(1)}, bf16[64]{0:T(256)(128)(2,1)}, u32[]{:S(2)}) copy-start(bf16[64]{0:T(256)(128)(2,1)} %param.31) | copy-start | bytes 388
  5.9 5.2 %copy-start.3 = (f32[24,8]{0,1:T(8,128)}, f32[24,8]{0,1:T(8,128)S(1)}, u32[]{:S(2)}) copy-start(f32[24,8]{0,1:T(8,128)S(1)} %fusion.32) | copy-start | bytes 2308
  8.4 2.7 %copy-start.10 = (bf16[64]{0:T(256)(128)(2,1)S(1)}, bf16[64]{0:T(256)(128)(2,1)}, u32[]{:S(2)}) copy-start(bf16[64]{0:T(256)(128)(2,1)} %param.32) | copy-start | bytes 388
  8.5 2.7 %copy-start.1 = (bf16[24,2048]{1,0:T(8,128)(2,1)S(1)}, bf16[24,2048]{1,0:T(8,128)(2,1)}, u32[]{:S(2)}) copy-start(bf16[24,2048]{1,0:T(8,128)(2,1)} %tok_ref.1) | copy-start | bytes 294916
  8.5 2.7 %copy-start.2 = (bf16[2048,128]{1,0:T(8,128)(2,1)S(1)}, bf16[2048,128]{1,0:T(8,128)(2,1)}, u32[]{:S(2)}) copy-start(bf16[2048,128]{1,0:T(8,128)(2,1)} %param.27) | copy-start | bytes 1572868
  15.5 3.9 %copy-start.4 = (bf16[2048]{0:T(1024)(128)(2,1)S(1)}, bf16[2048]{0:T(1024)(128)(2,1)}, u32[]{:S(2)}) copy-start(bf16[2048]{0:T(1024)(128)(2,1)} %param.38) | copy-start | bytes 12292
  15.5 4.5 %copy-start.5 = (bf16[2048]{0:T(1024)(128)(2,1)S(1)}, bf16[2048]{0:T(1024)(128)(2,1)}, u32[]{:S(2)}) copy-start(bf16[2048]{0:T(1024)(128)(2,1)} %param.39) | copy-start | bytes 12292
  15.5 5.1 %copy-start.6 = (s32[24,2]{0,1:T(2,128)S(1)}, s32[24,2]{0,1:T(2,128)}, u32[]{:S(2)}) copy-start(s32[24,2]{0,1:T(2,128)} %param.43) | copy-start | bytes 580
  15.5 5.8 %copy-start.7 = (f32[24,2]{0,1:T(2,128)S(1)}, f32[24,2]{0,1:T(2,128)}, u32[]{:S(2)}) copy-start(f32[24,2]{0,1:T(2,128)} %param.44) | copy-start | bytes 580
